TPU v7x, 256 devices: a 4x2x16 block of a 4x16x16 slice. The times are simulated.
256 devices in a mesh: grp: 2 (over y), sp: 16 (over z), tp: 8 (over x, core).
Axes of the slice: x: 4, y: 2, z: 16, core: 2. Of those that a mesh axis runs over, the one named last changes fastest.
The devices are a block of a 4x16x16 slice.
Arguments:
- tokens: bfloat16 [2, 16384, 2048], P('grp', ('sp', 'tp')), parts along dimension 0, may hold values from -6 to 6
- norm_gain: bfloat16 [2048], replicated, may hold values from 0.099609375 to 1.8984375
- w_query: bfloat16 [2048, 1024], P('sp'), may hold values from -0.125 to 0.125
- w_forget: bfloat16 [2048, 1024], P('sp'), may hold values from -0.125 to 0.125
- w_input: bfloat16 [2048, 1024], P('sp'), may hold values from -0.125 to 0.125
- floor_gap: float32 [1024], replicated, may hold values from 1.8310547e-05 to 0.12
- extra_decay: float32 [2, 16384, 16], P('grp', ('sp', 'tp')), parts along dimension 0, may hold values from -1.4 to 0, as said below
- init_state: float32 [2, 16, 64, 64], P('grp'), parts along dimension 0, may hold values from -0.03125 to 0.03125
- head_norm_gain: bfloat16 [1024], replicated, may hold values from 0.099609375 to 1.8984375
- w_output: bfloat16 [1024, 2048], P(None, 'sp'), may hold values from -0.1875 to 0.1875
Outputs:
- mixed: bfloat16 [2, 16384, 2048], P('grp', ('sp', 'tp')), parts along dimension 0
- final_state: float32 [2, 65536], P('grp', ('sp', 'tp')), parts along dimension 0
There are 2 independent parts, one for each index of `grp`. A program takes and returns all parts, laid end to end along the dimension named above; an argument that names none is the same for every part. Nothing has to cross between parts.
Inputs may be any that keep to these rules, and one draw needn't show every extreme that they name: `extra_decay`: no entry is positive.
All inputs are finite; a program needn't handle non-finite values.
Results may differ from a plain program's by a relative error of at most 0.014.
Values may be sent and summed in bfloat16 or wider, within the bound.
A program may use at most 128 MiB of HBM per device.

v0:
```python
import jax
import jax.numpy as jnp
from jax import lax
from jax.sharding import Mesh
from jax.sharding import PartitionSpec as P

HEADS = 16
HEAD = 64
BLOCK = 64
SP_TP = ("sp", "tp_0", "tp_1")
EPSILON = 1e-05


def nothing_yet(value, identity):
    return jax.tree.map(
        lambda a, e: jnp.broadcast_to(jnp.asarray(e, a.dtype), a.shape), value, identity
    )


def entering_2(value, axes, combine, identity):
    before = start = nothing_yet(value, identity)
    total = value
    for axis in reversed(axes):
        peers, mine = (lax.axis_size(axis), lax.axis_index(axis))
        pieces = jax.tree.map(
            lambda part, kind: lax.all_gather(part.astype(kind), axis),
            total,
            (jnp.bfloat16, jnp.bfloat16),
        )
        inside, total = (start, start)
        for k in range(peers):
            passed = k < mine
            total = combine(
                total, jax.tree.map(lambda part, own: part[k].astype(own.dtype), pieces, value)
            )
            inside = jax.tree.map(lambda new, old: jnp.where(passed, new, old), total, inside)
        before = combine(inside, before)
    return before


def prefix_by_axis(value, axes, combine, identity):
    before = start = nothing_yet(value, identity)
    total = value
    for axis in reversed(axes):
        peers, mine = (lax.axis_size(axis), lax.axis_index(axis))
        pieces = lax.all_gather(total, axis)
        inside, total = (start, start)
        for k in reversed(range(peers)):
            passed = k > mine
            total = combine(total, pieces[k])
            inside = jnp.where(passed, total, inside)
        before = combine(inside, before)
    return before


def reduced_to_own(pieces, axes, order):
    inside = pieces.shape[1:]
    pieces = pieces.reshape(*(lax.axis_size(a) for a in axes), *inside)
    pieces = jnp.moveaxis(pieces, order, range(len(axes))).reshape(-1, *inside)
    for k in order:
        pieces = lax.psum_scatter(pieces, axes[k], scatter_dimension=0, tiled=True)
    return pieces[0]


def in_blocks(value, dim, peers):
    lengths = value.shape
    pieces = value.reshape(*lengths[:dim], peers, lengths[dim] // peers, *lengths[dim + 1 :])
    return jnp.moveaxis(pieces, dim, 0)


def summed_rows(value, axes, order, dim):
    peers = lax.axis_size(axes)
    return reduced_to_own(in_blocks(value, dim, peers), axes, order)


def layer_normed(tokens, norm_gain):
    values = tokens.astype(jnp.float32)
    center = values - jnp.mean(values, axis=-1, keepdims=True)
    spread = jnp.mean(center * center, axis=-1, keepdims=True)
    return (center * lax.rsqrt(spread + EPSILON) * norm_gain.astype(jnp.float32)).astype(
        jnp.bfloat16
    )


def gate_terms(query_sum, forget_sum, input_sum, floor_gap, extra_decay):
    query_raw = query_sum.astype(jnp.bfloat16)
    forget_raw = forget_sum.astype(jnp.bfloat16)
    input_raw = input_sum.astype(jnp.bfloat16)
    forget_pre = forget_raw.astype(jnp.float32)
    split_shape = forget_pre.shape[:-1] + (HEADS, HEAD)
    log_keep = jnp.logaddexp(
        jnp.log1p(-floor_gap), jnp.log(floor_gap) + jax.nn.log_sigmoid(forget_pre)
    )
    log_keep = log_keep.reshape(split_shape) + extra_decay[..., None]
    key_gate = (floor_gap * jax.nn.sigmoid(-forget_pre)).reshape(split_shape)
    query = jax.nn.silu(query_raw.astype(jnp.float32)).reshape(split_shape)
    values = input_raw.astype(jnp.float32).reshape(split_shape)
    return (query, key_gate, values, log_keep)


def block_pass(query, key_gate, values, log_keep):
    highest = lax.Precision.HIGHEST
    cumul = jnp.cumsum(log_keep, axis=2)
    q_decayed = query * jnp.exp(cumul)
    key_decayed = key_gate * jnp.exp(-cumul)
    causal = lax.broadcasted_iota(jnp.int32, (BLOCK, BLOCK), 0) >= lax.broadcasted_iota(
        jnp.int32, (BLOCK, BLOCK), 1
    )
    scores = jnp.einsum("snthd,snuhd->snhtu", q_decayed, key_decayed, precision=highest)
    scores = jnp.where(causal, scores, 0.0)
    within = jnp.einsum("snhtu,snuhe->snthe", scores, values, precision=highest)
    totals = cumul[:, :, -1]
    k_tail = key_gate * jnp.exp(totals[:, :, None] - cumul)
    block_state = jnp.einsum("snthd,snthe->snhde", k_tail, values, precision=highest)
    return (q_decayed, within, totals, block_state)


def linked_advance(earlier, later):
    return (earlier[0] + later[0], jnp.exp(later[0])[..., None] * earlier[1] + later[1])


def add_logs(earlier, later):
    return earlier + later


def read_out(q_global, leading_logarithm, prefix_state, init_part):
    carried = jnp.exp(leading_logarithm)[..., None] * init_part + prefix_state
    added = jnp.einsum("snthd,shde->snthe", q_global, carried, precision=lax.Precision.HIGHEST)
    return (carried, added)


def body(
    tokens,
    norm_gain,
    w_query,
    w_forget,
    w_input,
    floor_gap,
    extra_decay,
    init_state,
    head_norm_gain,
    w_output,
):
    normed = layer_normed(tokens, norm_gain)
    seqs, span = (tokens.shape[0], tokens.shape[1])

    def add_rows(piece):
        return jnp.dot(normed, piece, preferred_element_type=jnp.float32)

    query_sum = add_rows(lax.all_gather(w_query, "sp", axis=0, tiled=True))
    forget_sum = add_rows(lax.all_gather(w_forget, "sp", axis=0, tiled=True))
    input_sum = add_rows(lax.all_gather(w_input, "sp", axis=0, tiled=True))
    query, key_gate, values, log_keep = gate_terms(
        query_sum, forget_sum, input_sum, floor_gap, extra_decay
    )
    blocks = span // BLOCK
    blocked = (seqs, blocks, BLOCK, HEADS, HEAD)
    q_decayed, within, totals, block_state = block_pass(
        query.reshape(blocked),
        key_gate.reshape(blocked),
        values.reshape(blocked),
        log_keep.reshape(blocked),
    )
    running_state = jnp.zeros((seqs, HEADS, HEAD, HEAD), jnp.float32)
    running_log = jnp.zeros((seqs, HEADS, HEAD), jnp.float32)
    entering_list = []
    offset_list = []
    for number in range(blocks):
        entering_list.append(running_state)
        offset_list.append(running_log)
        running_state = (
            jnp.exp(totals[:, number])[..., None] * running_state + block_state[:, number]
        )
        running_log = running_log + totals[:, number]
    entering = jnp.stack(entering_list, axis=1)
    offsets = jnp.stack(offset_list, axis=1)
    local_out = within + jnp.einsum(
        "snthd,snhde->snthe", q_decayed, entering, precision=lax.Precision.HIGHEST
    )
    q_global = q_decayed * jnp.exp(offsets[:, :, None])
    leading_logarithm, prefix_state = entering_2(
        (running_log, running_state),
        SP_TP,
        linked_advance,
        (jnp.zeros_like(running_log), jnp.zeros_like(running_state)),
    )
    carried, added = read_out(q_global, leading_logarithm, prefix_state, init_state)
    flat_total = HEADS * HEAD * HEAD
    piece_count = flat_total // lax.axis_size(SP_TP)
    piece_start = lax.axis_index(SP_TP) * piece_count
    later_log = prefix_by_axis(running_log, SP_TP, add_logs, jnp.zeros_like(running_log))
    surviving = (jnp.exp(later_log)[..., None] * running_state).reshape(seqs, flat_total)
    summed = summed_rows(surviving.astype(jnp.bfloat16), SP_TP, (2, 0, 1), 1).astype(jnp.float32)
    initial_part = (
        jnp.exp(leading_logarithm + running_log + later_log)[..., None] * init_state
    ).reshape(seqs, flat_total)
    final_state = lax.dynamic_slice_in_dim(initial_part, piece_start, piece_count, 1) + summed
    recurrent = (local_out + added).reshape(seqs, span, HEADS, HEAD)
    average_power = jnp.mean(recurrent * recurrent, axis=-1, keepdims=True)
    scaled = (
        recurrent
        * lax.rsqrt(average_power + EPSILON)
        * head_norm_gain.astype(jnp.float32).reshape(HEADS, HEAD)
    )
    gated = scaled.reshape(seqs, span, HEADS * HEAD).astype(jnp.bfloat16)
    mixed = jnp.dot(
        gated,
        lax.all_gather(w_output, "sp", axis=1, tiled=True),
        preferred_element_type=jnp.float32,
    ).astype(jnp.bfloat16)
    return (mixed, final_state)


def solution(mesh):
    torus = Mesh(
        mesh.devices.reshape(mesh.shape["grp"], mesh.shape["sp"], 4, 2),
        ("grp", "sp", "tp_0", "tp_1"),
    )
    in_specs = (
        P("grp", SP_TP, None),
        P(),
        P("sp", None),
        P("sp", None),
        P("sp", None),
        P(),
        P("grp", SP_TP, None),
        P("grp", None, None, None),
        P(),
        P(None, "sp"),
    )
    out_specs = (P("grp", SP_TP, None), P("grp", SP_TP))
    return jax.shard_map(body, mesh=torus, in_specs=in_specs, out_specs=out_specs, check_vma=False)
```

profile of v0, /device:TPU:36, one launch (start us, length us, event | category | flops | bytes accessed | tf_op | source)
XLA Modules:
  0.0 588.2 jit_solution(18242492222280507001)
XLA Ops:
  7.2 0.7 all-gather.10.cloned.1.call-update
  8.0 0.7 all-gather.8.cloned.1.call-update
  8.8 0.7 all-gather.6.cloned.1.call-update
  9.7 0.7 convert_element_type.904
  10.4 0.8 copy.81
  11.2 1.2 convert_reduce_fusion
  12.4 1.3 fusion.7
  13.8 0.7 negate_log-plus-one_fusion
  14.5 85.1 %all-gather.10.cloned.1.call-done = bf16[2048,1024]{1,0:T(8,128)(2,1)} async-done(((bf16[128,1024]{1,0:T(8,128)(2,1)}), bf16[2048,1024]{1,0:T(8,128)(2,1)}) %all-gather.10.cloned.1.call-update) | async-done | bytes 4194320 | tf_op jit(solution)/shard_map/all_gather | solution.py:151
  99.6 3.8 add_select_fusion
  104.2 1.9 all_gather.51
  106.1 1.9 all_gather.58
  108.5 10.8 %all_gather.52 = bf16[4,1,16,64]{3,2,1,0:T(8,128)(2,1)S(1)} all-gather(bf16[1,1,16,64]{3,2,1,0:T(8,128)(2,1)S(1)} %get-tuple-element.47), channel_id=1, replica_groups=mesh['grp'=2,'sp'=16,'tp_0'=4,'tp_1'=2] {'tp_0'}, dimensions={0}, use_global_device_ids=true | all-gather | bytes 10240 | tf_op jit(solution)/shard_map/all_gather | solution.py:26
  119.4 11.9 %all_gather.59 = f32[4,1,16,64]{3,2,1,0:T(8,128)S(1)} all-gather(f32[1,1,16,64]{3,2,1,0:T(8,128)S(1)} %slice_add_fusion.18), channel_id=1, replica_groups=mesh['grp'=2,'sp'=16,'tp_0'=4,'tp_1'=2] {'tp_0'}, dimensions={0}, use_global_device_ids=true | all-gather | bytes 20480 | tf_op jit(solution)/shard_map/all_gather | solution.py:46
  131.3 29.1 %all_gather.53 = bf16[16,1,16,64]{3,2,1,0:T(8,128)(2,1)S(1)} all-gather(bf16[1,1,16,64]{3,2,1,0:T(8,128)(2,1)S(1)} %get-tuple-element.37), channel_id=1, replica_groups=mesh['grp'=2,'sp'=16,'tp_0'=4,'tp_1'=2] {'sp'}, dimensions={0}, use_global_device_ids=true | all-gather | bytes 34816 | tf_op jit(solution)/shard_map/all_gather | solution.py:26
  160.4 26.9 %all_gather.60 = f32[16,1,16,64]{3,2,1,0:T(8,128)S(1)} all-gather(f32[1,1,16,64]{3,2,1,0:T(8,128)S(1)} %slice_add_fusion.15), channel_id=1, replica_groups=mesh['grp'=2,'sp'=16,'tp_0'=4,'tp_1'=2] {'sp'}, dimensions={0}, use_global_device_ids=true | all-gather | bytes 69632 | tf_op jit(solution)/shard_map/all_gather | solution.py:46
  187.3 0.7 fusion.207
  188.4 1.3 reshape_reshape.8
  189.7 3.1 divide_multiply_fusion.1
  192.8 1.2 reshape_reshape.7
  194.0 55.5 %all-gather.6.cloned.1.call-done = bf16[2048,1024]{1,0:T(8,128)(2,1)} async-done(((bf16[128,1024]{1,0:T(8,128)(2,1)}), bf16[2048,1024]{1,0:T(8,128)(2,1)}) %all-gather.6.cloned.1.call-update) | async-done | bytes 4194320 | tf_op jit(solution)/shard_map/all_gather | solution.py:152
  249.5 3.0 convolution_convert_fusion.3
  252.8 3.3 fusion.16
  256.1 1.2 convolution_bitcast_fusion.1
  257.3 1.2 add_convert_fusion
  259.1 0.9 mul.695
  260.2 0.9 mul.697
  261.2 1.5 fusion.154
  262.8 0.7 reshape.2017
  263.6 2.6 all_gather.54
  266.6 14.0 %all_gather.55 = bf16[4,1,16,64,64]{4,3,2,1,0:T(8,128)(2,1)} all-gather(bf16[1,1,16,64,64]{4,3,2,1,0:T(8,128)(2,1)S(1)} %fusion.36), channel_id=1, replica_groups=mesh['grp'=2,'sp'=16,'tp_0'=4,'tp_1'=2] {'tp_0'}, dimensions={0}, use_global_device_ids=true | all-gather | bytes 655360 | tf_op jit(solution)/shard_map/all_gather | solution.py:26
  280.7 2.5 fusion.52
  283.3 0.7 all-gather.14.cloned.1.call-update
  284.0 1.3 dynamic-slice
  287.2 2.0 broadcast_multiply_fusion.1
  289.2 1.4 reshape.2016
  291.8 2.4 convolution_select_fusion
  294.2 1.0 fusion.96
  295.3 3.0 fusion.1
  298.3 114.6 %all-reduce.6.cloned.1.call-done = bf16[64,1,512]{2,0,1:T(8,128)(2,1)} async-done(((bf16[64,1,512]{2,0,1:T(8,128)(2,1)}), bf16[64,1,512]{2,0,1:T(8,128)(2,1)}) %all-reduce.6.cloned.1.call-update) | async-done | bytes 65552
  412.9 0.7 constant_dynamic-slice_fusion
  413.6 8.3 %all-reduce.3 = bf16[4,1,512]{2,0,1:T(4,128)(2,1)S(1)} all-reduce(bf16[4,1,512]{2,0,1:T(4,128)(2,1)S(1)} %constant_dynamic-slice_fusion), channel_id=4, replica_groups=mesh['grp'=2,'sp'=16,'tp_0'=4,'tp_1'=2] {'tp_0'}, use_global_device_ids=true, to_apply=%region_6.7.clone | all-reduce | flops 2048 | bytes 8192
  421.9 1.2 convert_add_fusion.55
  423.1 63.5 %all-gather.12.cloned.1.call-done = bf16[16,1,16,64,64]{4,3,2,1,0:T(8,128)(2,1)} async-done(((bf16[1,1,16,64,64]{4,3,2,1,0:T(8,128)(2,1)}), bf16[16,1,16,64,64]{4,3,2,1,0:T(8,128)(2,1)}) %all-gather.12.cloned.1.call-update) | async-done | bytes 2097168 | tf_op jit(solution)/shard_map/all_gather | solution.py:26
  486.6 10.3 %multiply_reduce_fusion = (f32[2,64,16]{1,2,0:T(8,128)S(1)}, f32[1,2,64,16,64]{2,4,3,1,0:T(8,128)}) fusion(f32[1,2,64,16,64]{2,4,3,1,0:T(8,128)} %fusion.1, f32[2,64,16,64]{3,2,1,0:T(8,128)S(1)} %copy-done.3, f32[1,16,64,64]{3,2,1,0:T(8,128)} %param.17, bf16[16,1,16,64,64]{4,3,2,1,0:T(8,128)(2,1)} %all-gather.12.cloned.1.call-done, ...), kind=kOutput, calls=%fused_computation.33 | convolution fusion | flops 107018240 | bytes 4829206 | tf_op jit(solution)/shard_map/snthd,shde->snthe/dot_general | solution.py:128
  497.0 1.7 copy.73
  499.4 78.2 %all-gather.14.cloned.1.call-done = bf16[1024,2048]{1,0:T(8,128)(2,1)} async-done(((bf16[1024,128]{1,0:T(8,128)(2,1)}), bf16[1024,2048]{1,0:T(8,128)(2,1)}) %all-gather.14.cloned.1.call-update) | async-done | bytes 4194320 | tf_op jit(solution)/shard_map/all_gather | solution.py:208
  577.6 3.7 fusion
  (80 shorter events, 7.1 us)
Async XLA Ops:
  7.2 92.5 %all-gather.10.cloned.1.call-start = ((), (), s32[]{:S(2)}) async-start(), calls=%async_computation.3 | async-start | bytes 4456448 | tf_op jit(solution)/shard_map/all_gather | solution.py:151
  8.0 181.7 %all-gather.8.cloned.1.call-start = ((), (), s32[]{:S(2)}) async-start(), calls=%async_computation.2 | async-start | bytes 4456448 | tf_op jit(solution)/shard_map/all_gather | solution.py:150
  8.8 240.7 %all-gather.6.cloned.1.call-start = ((), (), s32[]{:S(2)}) async-start(), calls=%async_computation.1 | async-start | bytes 4456448 | tf_op jit(solution)/shard_map/all_gather | solution.py:152
  9.6 271.0 %reduce-scatter.4.cloned.1.call-start = ((), (), s32[]{:S(2)}) async-start(), calls=%async_computation.6 | async-start | bytes 196608 | tf_op jit(solution)/shard_map/reduce_scatter | solution.py:61
  10.4 93.0 %copy-start.9 = (f32[2048]{0:T(1024)}, f32[2048]{0:T(1024)S(1)}, u32[]{:S(2)}) copy-start(f32[2048]{0:T(1024)S(1)} %convert_element_type.904) | copy-start | bytes 24580
  12.4 91.0 %copy-start.12 = (f32[128]{0:T(128)}, f32[128]{0:T(128)S(1)}, u32[]{:S(2)}) copy-start(f32[128]{0:T(128)S(1)} %broadcast_multiply_fusion.2) | copy-start | bytes 1540
  13.8 89.7 %copy-start.15 = (f32[128]{0:T(128)}, f32[128]{0:T(128)S(1)}, u32[]{:S(2)}) copy-start(f32[128]{0:T(128)S(1)} %add_rsqrt_fusion.1) | copy-start | bytes 1540
  103.4 86.3 %copy-start.1 = (bf16[1,128,2048]{2,1,0:T(8,128)(2,1)S(1)}, bf16[1,128,2048]{2,1,0:T(8,128)(2,1)}, u32[]{:S(2)}) copy-start(bf16[1,128,2048]{2,1,0:T(8,128)(2,1)} %param.10) | copy-start | bytes 1572868
  189.7 59.8 %copy-start.10 = (f32[2048]{0:T(1024)S(1)}, f32[2048]{0:T(1024)}, u32[]{:S(2)}) copy-start(f32[2048]{0:T(1024)} %copy-done.9) | copy-start | bytes 24580
  189.7 59.8 %copy-start.13 = (f32[128]{0:T(128)S(1)}, f32[128]{0:T(128)}, u32[]{:S(2)}) copy-start(f32[128]{0:T(128)} %copy-done.12) | copy-start | bytes 1540
  189.7 59.8 %copy-start.16 = (f32[128]{0:T(128)S(1)}, f32[128]{0:T(128)}, u32[]{:S(2)}) copy-start(f32[128]{0:T(128)} %copy-done.15) | copy-start | bytes 1540
  260.0 27.1 %copy-start.4 = (f32[16,64]{1,0:T(8,128)S(1)}, f32[16,64]{1,0:T(8,128)}, u32[]{:S(2)}) copy-start(f32[16,64]{1,0:T(8,128)} %get-tuple-element.2) | copy-start | bytes 12292
  260.2 25.1 %copy-start.14 = (u32[256]{0:T(256)S(1)}, u32[256]{0:T(256)}, u32[]{:S(2)}) copy-start(u32[256]{0:T(256)} %constant.88) | copy-start | bytes 3076
  260.2 25.7 %copy-start.11 = (bf16[1024]{0:T(1024)(128)(2,1)S(1)}, bf16[1024]{0:T(1024)(128)(2,1)}, u32[]{:S(2)}) copy-start(bf16[1024]{0:T(1024)(128)(2,1)} %param.18) | copy-start | bytes 6148
  261.2 29.4 %copy-start.6 = (f32[16,64]{1,0:T(8,128)S(1)}, f32[16,64]{1,0:T(8,128)}, u32[]{:S(2)}) copy-start(f32[16,64]{1,0:T(8,128)} %get-tuple-element.4) | copy-start | bytes 12292
  261.2 30.0 %copy-start.5 = (f32[16,64]{1,0:T(8,128)S(1)}, f32[16,64]{1,0:T(8,128)}, u32[]{:S(2)}) copy-start(f32[16,64]{1,0:T(8,128)} %get-tuple-element.5) | copy-start | bytes 12292
  261.2 30.6 %copy-start = (f32[2,64,16,64]{3,2,1,0:T(8,128)S(1)}, f32[2,64,16,64]{3,2,1,0:T(8,128)}, u32[]{:S(2)}) copy-start(f32[2,64,16,64]{3,2,1,0:T(8,128)} %get-tuple-element.13) | copy-start | bytes 1572868
  263.5 149.4 %all-reduce.6.cloned.1.call-start = ((), (), s32[]{:S(2)}) async-start(), calls=%async_computation.7 | async-start | bytes 131072
  280.6 206.0 %all-gather.12.cloned.1.call-start = ((), (), s32[]{:S(2)}) async-start(), calls=%async_computation.4 | async-start | bytes 4456448 | tf_op jit(solution)/shard_map/all_gather | solution.py:26
  283.2 294.4 %all-gather.14.cloned.1.call-start = ((), (), s32[]{:S(2)}) async-start(), calls=%async_computation.5 | async-start | bytes 4456448 | tf_op jit(solution)/shard_map/all_gather | solution.py:208
  290.6 4.7 copy-start.2
  291.8 194.8 %copy-start.8 = (f32[16,64]{1,0:T(8,128)S(1)}, f32[16,64]{1,0:T(8,128)}, u32[]{:S(2)}) copy-start(f32[16,64]{1,0:T(8,128)} %get-tuple-element.45) | copy-start | bytes 12292
  294.2 192.4 %copy-start.3 = (f32[2,64,16,64]{3,2,1,0:T(8,128)S(1)}, f32[2,64,16,64]{3,2,1,0:T(8,128)}, u32[]{:S(2)}) copy-start(f32[2,64,16,64]{3,2,1,0:T(8,128)} %get-tuple-element.16) | copy-start | bytes 1572868
  496.9 80.7 %copy-start.7 = (f32[1024]{0:T(1024)S(1)}, f32[1024]{0:T(1024)}, u32[]{:S(2)}) copy-start(f32[1024]{0:T(1024)} %convert_element_type.1001) | copy-start | bytes 12292
Sparse Core Ops, SparseCore 0:
  9.8 89.7 all-gather.9
  101.4 73.5 all-gather.7
  176.8 72.5 all-gather.5
  263.6 13.2 reduce-scatter.3
  280.7 132.1 all-reduce.5
  414.6 72.0 all-gather.11
  488.4 89.1 all-gather.13
where the time goes:
time: 589 us; the launch traced here: 588 us
  waiting for transfers between devices  400 us (68%)
  blocking collectives  107 us (18%)
  matrix products  31.4 us (5%)
  other arithmetic  18.4 us (3%)
  local copies, waits for them, and re-layouts  15.3 us (3%)
  between operations  15.2 us (3%)
    unnamed x8, waiting for transfers between devices  118 us
    all_gather x1, waiting for transfers between devices, body(): forget_sum = add_rows(lax.all_gather(w_forget, 'sp', axis=0, tiled=True))  85.1 us
    all_gather x1, waiting for transfers between devices, body(): lax.all_gather(w_output, 'sp', axis=1, tiled=True)  78.2 us
    all_gather x1, waiting for transfers between devices, entering_2(): lax.all_gather(part.astype(kind), axis)  63.5 us
    all_gather x5, blocking collectives, entering_2(): lax.all_gather(part.astype(kind), axis)  58.3 us
    all_gather x1, waiting for transfers between devices, body(): input_sum = add_rows(lax.all_gather(w_input, 'sp', axis=0, tiled=True))  55.5 us
    all_gather x3, blocking collectives, prefix_by_axis(): pieces = lax.all_gather(total, axis)  40.7 us
  transfers between devices with their start and end apart: 7, of which 5 were waited for; matrix products, arithmetic and copies ran while one was open for 8% of the time, Pallas kernels for 0%

commit v1 on v0

--- a/solution.py
+++ b/solution.py
@@ -1,3 +1,4 @@
+import functools
 import jax
 import jax.numpy as jnp
 from jax import lax
@@ -9,6 +10,15 @@
 BLOCK = 64
 SP_TP = ("sp", "tp_0", "tp_1")
 EPSILON = 1e-05
+
+
+def modes_deliver(raw, in_dim):
+    right_arr = lax.axis_size("sp")
+    view_out = jnp.concatenate(right_arr * [raw], in_dim)
+    return lax.all_to_all(view_out, "sp", in_dim, in_dim, tiled=True)
+
+
+store_rates_now = functools.partial(modes_deliver, in_dim=1)
 
 
 def nothing_yet(value, identity):
@@ -203,11 +213,9 @@
         * head_norm_gain.astype(jnp.float32).reshape(HEADS, HEAD)
     )
     gated = scaled.reshape(seqs, span, HEADS * HEAD).astype(jnp.bfloat16)
-    mixed = jnp.dot(
-        gated,
-        lax.all_gather(w_output, "sp", axis=1, tiled=True),
-        preferred_element_type=jnp.float32,
-    ).astype(jnp.bfloat16)
+    mixed = jnp.dot(gated, store_rates_now(w_output), preferred_element_type=jnp.float32).astype(
+        jnp.bfloat16
+    )
     return (mixed, final_state)
 
 

time: 589 us -> 769 us (1.31)
  waiting for transfers between devices: 400 us -> 543 us
  starting transfers between devices: 0.44 us -> 24.5 us
  local copies, waits for them, and re-layouts: 15.3 us -> 30 us
    all_gather x1, waiting for transfers between devices: 85.1 us -> 221 us  [body(): forget_sum = add_rows(lax.all_gather(w_forget, 'sp', axis=0, tiled=True))]
    all_gather x1 -> x0, waiting for transfers between devices: 78.2 us -> none  [body(): lax.all_gather(w_output, 'sp', axis=1, tiled=True)]
    all_gather x1, waiting for transfers between devices: 0.01 us -> 72.4 us  [body(): query_sum = add_rows(lax.all_gather(w_query, 'sp', axis=0, tiled=True))]
    all_to_all x0 -> x1, starting transfers between devices: none -> 24.1 us  [modes_deliver(): return lax.all_to_all(view_out, 'sp', in_dim, in_dim, tiled=True)]
    all_gather x1, waiting for transfers between devices: 55.5 us -> 70.5 us  [body(): input_sum = add_rows(lax.all_gather(w_input, 'sp', axis=0, tiled=True))]
    all_to_all x0 -> x2, local copies, waits for them, and re-layouts: none -> 12.9 us  [modes_deliver(): return lax.all_to_all(view_out, 'sp', in_dim, in_dim, tiled=True)]
    unnamed x8 -> x7, waiting for transfers between devices: 118 us -> 116 us
where the time goes in v1:
time: 769 us; the launch traced here: 768 us
  waiting for transfers between devices  543 us (71%)
  blocking collectives  109 us (14%)
  matrix products  31.3 us (4%)
  local copies, waits for them, and re-layouts  30 us (4%)
  starting transfers between devices  24.5 us (3%)
  between operations  15.4 us (2%)
  other arithmetic  14.5 us (2%)
    all_gather x1, waiting for transfers between devices, body(): forget_sum = add_rows(lax.all_gather(w_forget, 'sp', axis=0, tiled=True))  221 us
    unnamed x7, waiting for transfers between devices  116 us
    all_gather x1, waiting for transfers between devices, body(): query_sum = add_rows(lax.all_gather(w_query, 'sp', axis=0, tiled=True))  72.4 us
    all_gather x1, waiting for transfers between devices, body(): input_sum = add_rows(lax.all_gather(w_input, 'sp', axis=0, tiled=True))  70.5 us
    all_gather x1, waiting for transfers between devices, entering_2(): lax.all_gather(part.astype(kind), axis)  63.4 us
    all_gather x5, blocking collectives, entering_2(): lax.all_gather(part.astype(kind), axis)  59.6 us
    all_gather x3, blocking collectives, prefix_by_axis(): pieces = lax.all_gather(total, axis)  40.7 us
    all_to_all x1, starting transfers between devices, modes_deliver(): return lax.all_to_all(view_out, 'sp', in_dim, in_dim, tiled=True)  24.1 us
  transfers between devices with their start and end apart: 7, of which 5 were waited for; matrix products, arithmetic and copies ran while one was open for 8% of the time, Pallas kernels for 0%

profile of v1, /device:TPU:36, one launch (start us, length us, event | category | flops | bytes accessed | tf_op | source)
XLA Modules:
  0.0 767.8 jit_solution(6166079667572727115)
XLA Ops:
  7.2 0.7 all-gather.9.cloned.1.call-update
  8.0 0.7 all-gather.7.cloned.1.call-update
  8.8 0.7 all-gather.5.cloned.1.call-update
  9.6 1.1 copy.71
  11.1 1.9 copy-done
  13.0 6.4 copy.87
  19.5 24.1 %all-to-all-start = ((bf16[1024,16,128]{2,0,1:T(8,128)(2,1)}), bf16[1024,16,128]{2,0,1:T(8,128)(2,1)}, u32[]{:S(2)}, u32[]{:S(2)}) async-start(bf16[1024,16,128]{2,0,1:T(8,128)(2,1)} %copy.87), calls=%async_computation | async-start | bytes 8388608 | tf_op jit(solution)/shard_map/all_to_all | solution.py:18
  44.4 220.5 %all-gather.9.cloned.1.call-done = bf16[2048,1024]{1,0:T(8,128)(2,1)} async-done(((bf16[128,1024]{1,0:T(8,128)(2,1)}), bf16[2048,1024]{1,0:T(8,128)(2,1)}) %all-gather.9.cloned.1.call-update) | async-done | bytes 4194320 | tf_op jit(solution)/shard_map/all_gather | solution.py:161
  264.9 3.7 add_select_fusion
  268.6 1.3 reshape_reshape.8
  270.2 72.4 %all-gather.7.cloned.1.call-done = bf16[2048,1024]{1,0:T(8,128)(2,1)} async-done(((bf16[128,1024]{1,0:T(8,128)(2,1)}), bf16[2048,1024]{1,0:T(8,128)(2,1)}) %all-gather.7.cloned.1.call-update) | async-done | bytes 4194320 | tf_op jit(solution)/shard_map/all_gather | solution.py:160
  342.6 3.0 divide_multiply_fusion.1
  345.6 1.3 reshape_reshape.7
  346.8 70.5 %all-gather.5.cloned.1.call-done = bf16[2048,1024]{1,0:T(8,128)(2,1)} async-done(((bf16[128,1024]{1,0:T(8,128)(2,1)}), bf16[2048,1024]{1,0:T(8,128)(2,1)}) %all-gather.5.cloned.1.call-update) | async-done | bytes 4194320 | tf_op jit(solution)/shard_map/all_gather | solution.py:162
  417.4 2.9 convolution_convert_fusion.3
  421.1 1.9 all_gather.48
  423.0 1.9 all_gather.54
  425.5 10.8 %all_gather.49 = bf16[4,1,16,64]{3,2,1,0:T(8,128)(2,1)S(1)} all-gather(bf16[1,1,16,64]{3,2,1,0:T(8,128)(2,1)S(1)} %get-tuple-element.47), channel_id=1, replica_groups=mesh['grp'=2,'sp'=16,'tp_0'=4,'tp_1'=2] {'tp_0'}, dimensions={0}, use_global_device_ids=true | all-gather | bytes 10240 | tf_op jit(solution)/shard_map/all_gather | solution.py:36
  436.3 11.9 %all_gather.55 = f32[4,1,16,64]{3,2,1,0:T(8,128)S(1)} all-gather(f32[1,1,16,64]{3,2,1,0:T(8,128)S(1)} %slice_add_fusion.18), channel_id=1, replica_groups=mesh['grp'=2,'sp'=16,'tp_0'=4,'tp_1'=2] {'tp_0'}, dimensions={0}, use_global_device_ids=true | all-gather | bytes 20480 | tf_op jit(solution)/shard_map/all_gather | solution.py:56
  448.2 29.0 %all_gather.50 = bf16[16,1,16,64]{3,2,1,0:T(8,128)(2,1)S(1)} all-gather(bf16[1,1,16,64]{3,2,1,0:T(8,128)(2,1)S(1)} %get-tuple-element.37), channel_id=1, replica_groups=mesh['grp'=2,'sp'=16,'tp_0'=4,'tp_1'=2] {'sp'}, dimensions={0}, use_global_device_ids=true | all-gather | bytes 34816 | tf_op jit(solution)/shard_map/all_gather | solution.py:36
  477.3 26.9 %all_gather.56 = f32[16,1,16,64]{3,2,1,0:T(8,128)S(1)} all-gather(f32[1,1,16,64]{3,2,1,0:T(8,128)S(1)} %slice_add_fusion.15), channel_id=1, replica_groups=mesh['grp'=2,'sp'=16,'tp_0'=4,'tp_1'=2] {'sp'}, dimensions={0}, use_global_device_ids=true | all-gather | bytes 69632 | tf_op jit(solution)/shard_map/all_gather | solution.py:56
  504.2 0.6 fusion.206
  505.3 3.3 fusion.16
  508.6 1.2 convolution_bitcast_fusion.1
  509.8 1.2 add_convert_fusion
  511.9 0.9 mul.704
  512.8 0.9 squeeze.40
  513.7 1.5 fusion.153
  515.3 0.7 reshape.2021
  516.1 2.4 all_gather.51
  518.9 15.5 %all_gather.52 = bf16[4,1,16,64,64]{4,3,2,1,0:T(8,128)(2,1)} all-gather(bf16[1,1,16,64,64]{4,3,2,1,0:T(8,128)(2,1)S(1)} %fusion.36), channel_id=1, replica_groups=mesh['grp'=2,'sp'=16,'tp_0'=4,'tp_1'=2] {'tp_0'}, dimensions={0}, use_global_device_ids=true | all-gather | bytes 655360 | tf_op jit(solution)/shard_map/all_gather | solution.py:36
  534.5 2.5 fusion.52
  537.1 1.3 dynamic-slice
  539.6 1.3 exp.349
  540.9 0.6 exp.348
  541.5 2.0 broadcast_multiply_fusion.1
  543.6 1.4 reshape.2020
  545.0 2.4 convolution_select_fusion
  547.4 1.0 fusion.96
  548.4 3.0 fusion.1
  551.5 114.1 %all-reduce.6.cloned.1.call-done = bf16[64,1,512]{2,0,1:T(8,128)(2,1)} async-done(((bf16[64,1,512]{2,0,1:T(8,128)(2,1)}), bf16[64,1,512]{2,0,1:T(8,128)(2,1)}) %all-reduce.6.cloned.1.call-update) | async-done | bytes 65552
  665.6 0.7 constant_dynamic-slice_fusion
  666.3 8.5 %all-reduce.3 = bf16[4,1,512]{2,0,1:T(4,128)(2,1)S(1)} all-reduce(bf16[4,1,512]{2,0,1:T(4,128)(2,1)S(1)} %constant_dynamic-slice_fusion), channel_id=4, replica_groups=mesh['grp'=2,'sp'=16,'tp_0'=4,'tp_1'=2] {'tp_0'}, use_global_device_ids=true, to_apply=%region_6.7.clone | all-reduce | flops 2048 | bytes 8192
  674.8 1.1 convert_add_fusion.55
  675.9 63.4 %all-gather.11.cloned.1.call-done = bf16[16,1,16,64,64]{4,3,2,1,0:T(8,128)(2,1)} async-done(((bf16[1,1,16,64,64]{4,3,2,1,0:T(8,128)(2,1)}), bf16[16,1,16,64,64]{4,3,2,1,0:T(8,128)(2,1)}) %all-gather.11.cloned.1.call-update) | async-done | bytes 2097168 | tf_op jit(solution)/shard_map/all_gather | solution.py:36
  739.3 9.6 %multiply_reduce_fusion = (f32[2,64,16]{1,2,0:T(8,128)S(1)}, f32[1,2,64,16,64]{2,4,3,1,0:T(8,128)S(1)}) fusion(f32[1,2,64,16,64]{2,4,3,1,0:T(8,128)} %fusion.1, f32[2,64,16,64]{3,2,1,0:T(8,128)S(1)} %copy-done.4, f32[1,16,64,64]{3,2,1,0:T(8,128)} %param.17, bf16[16,1,16,64,64]{4,3,2,1,0:T(8,128)(2,1)} %all-gather.11.cloned.1.call-done, ...), kind=kOutput, calls=%fused_computation.34 | convolution fusion | flops 107018240 | bytes 4829206 | tf_op jit(solution)/shard_map/snthd,shde->snthe/dot_general | solution.py:138
  750.0 6.5 copy.88
  756.4 4.5 fusion
  (85 shorter events, 6.4 us)
Async XLA Ops:
  7.2 257.8 %all-gather.9.cloned.1.call-start = ((), (), s32[]{:S(2)}) async-start(), calls=%async_computation.4 | async-start | bytes 4456448 | tf_op jit(solution)/shard_map/all_gather | solution.py:161
  8.0 334.6 %all-gather.7.cloned.1.call-start = ((), (), s32[]{:S(2)}) async-start(), calls=%async_computation.3 | async-start | bytes 4456448 | tf_op jit(solution)/shard_map/all_gather | solution.py:160
  8.8 408.6 %all-gather.5.cloned.1.call-start = ((), (), s32[]{:S(2)}) async-start(), calls=%async_computation.2 | async-start | bytes 4456448 | tf_op jit(solution)/shard_map/all_gather | solution.py:162
  11.1 1.9 copy-start
  19.5 24.3 %copy-start.8 = (bf16[2048]{0:T(1024)(128)(2,1)S(1)}, bf16[2048]{0:T(1024)(128)(2,1)}, u32[]{:S(2)}) copy-start(bf16[2048]{0:T(1024)(128)(2,1)} %param.11) | copy-start | bytes 12292
  19.5 24.3 %copy-start.5 = (f32[1,128,16]{1,2,0:T(8,128)S(1)}, f32[1,128,16]{1,2,0:T(8,128)}, u32[]{:S(2)}) copy-start(f32[1,128,16]{1,2,0:T(8,128)} %param.16) | copy-start | bytes 24580
  19.5 24.4 %copy-start.2 = (bf16[1,128,2048]{2,1,0:T(8,128)(2,1)S(1)}, bf16[1,128,2048]{2,1,0:T(8,128)(2,1)}, u32[]{:S(2)}) copy-start(bf16[1,128,2048]{2,1,0:T(8,128)(2,1)} %param.10) | copy-start | bytes 1572868
  19.5 24.9 %copy-start.9 = (f32[1024]{0:T(1024)S(1)}, f32[1024]{0:T(1024)}, u32[]{:S(2)}) copy-start(f32[1024]{0:T(1024)} %param.15) | copy-start | bytes 12292
  19.5 730.4 %all-to-all-start = ((bf16[1024,16,128]{2,0,1:T(8,128)(2,1)}), bf16[1024,16,128]{2,0,1:T(8,128)(2,1)}, u32[]{:S(2)}, u32[]{:S(2)}) async-start(bf16[1024,16,128]{2,0,1:T(8,128)(2,1)} %copy.87), calls=%async_computation | async-start | bytes 8388608 | tf_op jit(solution)/shard_map/all_to_all | solution.py:18
  43.6 490.7 %reduce-scatter.4.cloned.1.call-start = ((), (), s32[]{:S(2)}) async-start(), calls=%async_computation.6 | async-start | bytes 196608 | tf_op jit(solution)/shard_map/reduce_scatter | solution.py:71
  511.8 25.2 %copy-start.10 = (bf16[1024]{0:T(1024)(128)(2,1)S(1)}, bf16[1024]{0:T(1024)(128)(2,1)}, u32[]{:S(2)}) copy-start(bf16[1024]{0:T(1024)(128)(2,1)} %param.18) | copy-start | bytes 6148
  511.8 26.5 %copy-start.11 = (u32[256]{0:T(256)S(1)}, u32[256]{0:T(256)}, u32[]{:S(2)}) copy-start(u32[256]{0:T(256)} %constant.88) | copy-start | bytes 3076
  513.7 31.2 %copy-start.1 = (f32[2,64,16,64]{3,2,1,0:T(8,128)S(1)}, f32[2,64,16,64]{3,2,1,0:T(8,128)}, u32[]{:S(2)}) copy-start(f32[2,64,16,64]{3,2,1,0:T(8,128)} %get-tuple-element.13) | copy-start | bytes 1572868
  516.0 149.5 %all-reduce.6.cloned.1.call-start = ((), (), s32[]{:S(2)}) async-start(), calls=%async_computation.7 | async-start | bytes 131072
  534.5 204.8 %all-gather.11.cloned.1.call-start = ((), (), s32[]{:S(2)}) async-start(), calls=%async_computation.5 | async-start | bytes 4456448 | tf_op jit(solution)/shard_map/all_gather | solution.py:36
  544.9 3.5 copy-start.3
  544.9 194.4 %copy-start.6 = (f32[16,64]{1,0:T(8,128)S(1)}, f32[16,64]{1,0:T(8,128)}, u32[]{:S(2)}) copy-start(f32[16,64]{1,0:T(8,128)} %get-tuple-element.45) | copy-start | bytes 12292
  545.0 194.4 %copy-start.7 = (f32[16,64]{1,0:T(8,128)S(1)}, f32[16,64]{1,0:T(8,128)}, u32[]{:S(2)}) copy-start(f32[16,64]{1,0:T(8,128)} %exp.349) | copy-start | bytes 12292
  547.4 191.9 %copy-start.4 = (f32[2,64,16,64]{3,2,1,0:T(8,128)S(1)}, f32[2,64,16,64]{3,2,1,0:T(8,128)}, u32[]{:S(2)}) copy-start(f32[2,64,16,64]{3,2,1,0:T(8,128)} %get-tuple-element.16) | copy-start | bytes 1572868
Sparse Core Ops, SparseCore 0:
  9.8 255.0 all-gather.8
  266.8 75.7 all-gather.6
  344.4 72.9 all-gather.4
  516.2 13.4 reduce-scatter.3
  534.6 130.9 all-reduce.5
  667.2 72.0 all-gather.10
